TPU v7x, 32 devices: a whole 2x2x4 slice. The times are simulated.
32 devices in a mesh: sp: 8 (over z, x), tp: 4 (over y, core).
Axes of the slice: x: 2, y: 2, z: 4, core: 2. Of those that a mesh axis runs over, the one named last changes fastest.
Arguments:
- resid: bfloat16 [3072, 2048], P('sp'), may hold values from -6 to 6
- cotangent: bfloat16 [3072, 2048], P('sp'), may hold values from -0.59765625 to 0.59765625
- routes: int32 [3072, 2], P('sp'), may hold values from 0 to 7, all different within a row; in each aligned block of 384 rows (0 to 383, 384 to 767, ...) at most 192 rows name the same one
- route_weight: float32 [3072, 2], P('sp'), may hold values from 0.3 to 2.2
- w_gate: bfloat16 [8, 2048, 1024], P('sp', None, 'tp'), may hold values from -0.125 to 0.125
- w_up: bfloat16 [8, 2048, 1024], P('sp', None, 'tp'), may hold values from -0.125 to 0.125
- w_down: bfloat16 [8, 1024, 2048], P('sp', 'tp'), may hold values from -0.1875 to 0.1875
- out_proj: bfloat16 [2048, 2816], P(None, 'tp'), may hold values from -0.109375 to 0.109375
- gate_pre: bfloat16 [3072, 2816], P('sp', 'tp'), may hold values from -8 to 8
- log_decay: float32 [3072, 2816], P('sp', 'tp'), may hold values from -1 to 0
- state_before: float32 [3072, 2816], P('sp', 'tp'), may hold values from -6 to 6
- step_input: bfloat16 [3072, 2816], P('sp', 'tp'), may hold values from -6 to 6
Outputs:
- grad_gate: float32 [8, 2048, 1024], P('sp', None, 'tp')
- grad_up: float32 [8, 2048, 1024], P('sp', None, 'tp')
- grad_down: float32 [8, 1024, 2048], P('sp', 'tp')
- grad_proj: float32 [2048, 2816], P('sp', 'tp')
- grad_gate_pre: bfloat16 [3072, 2816], P('sp', 'tp')
- grad_step_input: float32 [3072, 2816], P('sp', 'tp')
- grad_log_decay: float32 [3072, 2816], P('sp', 'tp')
Inputs may be any that keep to these rules, and one draw needn't show every extreme that they name: `routes`: each row names 2 different experts. In the rows of one device no expert is named more than 192 times; some expert is named exactly 192 times in the rows of some devices.
All inputs are finite; a program needn't handle non-finite values.
Results may differ from a plain program's by a relative error of at most 0.02.
Values may be sent and summed in bfloat16 or wider, within the bound.
A program may use at most 128 MiB of HBM per device.

v0:
```python
import jax
import jax.numpy as jnp
from jax import lax
from jax.sharding import PartitionSpec as P


def carried_in(part, axis, combine, identity):
    count = lax.axis_size(axis)
    place = lax.axis_index(axis)
    ahead = count - 1 - place
    gathered = jax.tree.map(lambda a: lax.all_gather(a, axis), part)
    state = jax.tree.map(lambda a, e: jnp.zeros_like(a) + jnp.asarray(e, a.dtype), part, identity)

    def one(turn, state):
        source = count - 1 - turn
        return combine(
            state, jax.tree.map(lambda a: lax.dynamic_index_in_dim(a, source, 0, False), gathered)
        )

    return lax.fori_loop(0, ahead, one, state)


def expert_work(in_rows, cot_rows, gate_w, up_w, down_w):
    gate_act = jnp.dot(in_rows, gate_w, preferred_element_type=jnp.float32)
    up_act = jnp.dot(in_rows, up_w, preferred_element_type=jnp.float32)
    sigmoid_a = jax.nn.sigmoid(gate_act)
    hidden = (jax.nn.silu(gate_act) * up_act).astype(jnp.bfloat16)
    grad_down = lax.dot_general(
        hidden, cot_rows, (((0,), (0,)), ((), ())), preferred_element_type=jnp.float32
    )
    d_hidden = lax.dot_general(
        cot_rows, down_w, (((1,), (1,)), ((), ())), preferred_element_type=jnp.float32
    )
    slope = sigmoid_a * (1.0 + gate_act * (1.0 - sigmoid_a))
    d_gate_act = (d_hidden * up_act * slope).astype(jnp.bfloat16)
    d_up_act = (d_hidden * jax.nn.silu(gate_act)).astype(jnp.bfloat16)
    grad_gate = lax.dot_general(
        in_rows, d_gate_act, (((0,), (0,)), ((), ())), preferred_element_type=jnp.float32
    )
    grad_up = lax.dot_general(
        in_rows, d_up_act, (((0,), (0,)), ((), ())), preferred_element_type=jnp.float32
    )
    partial_value = lax.dot_general(
        d_gate_act, gate_w, (((1,), (1,)), ((), ())), preferred_element_type=jnp.float32
    )
    partial_value = partial_value + lax.dot_general(
        d_up_act, up_w, (((1,), (1,)), ((), ())), preferred_element_type=jnp.float32
    )
    rounded = lax.optimization_barrier(partial_value.astype(jnp.bfloat16))
    return (grad_gate[None], grad_up[None], grad_down[None], rounded.astype(jnp.float32))


def gather_slots(resid_part, cot_part, slot_token, slot_weight, groups, capacity):
    col_width = resid_part.shape[1]
    resid_pad = jnp.concatenate([resid_part, jnp.zeros((1, col_width), jnp.bfloat16)], axis=0)
    cot_pad = jnp.concatenate([cot_part, jnp.zeros((1, col_width), jnp.bfloat16)], axis=0)
    send_rows = resid_pad[slot_token].reshape(groups, capacity, col_width)
    send_cot = (slot_weight[:, None] * cot_pad[slot_token].astype(jnp.float32)).astype(jnp.bfloat16)
    return (send_rows, send_cot.reshape(groups, capacity, col_width))


def combine_slots(returned, cot_part, slot_ids, tok_rows, top_count):
    col_width = returned.shape[2]
    flat_back = returned.reshape(-1, col_width)
    routed = jnp.sum(
        flat_back[slot_ids].astype(jnp.float32).reshape(tok_rows, top_count, col_width), axis=1
    )
    return (cot_part.astype(jnp.float32) + routed).astype(jnp.bfloat16)


def reverse_link(former, latter):
    return (former[0] * latter[0], latter[0] * former[1] + latter[1])


def compose(earlier, later):
    return (later[0] * earlier[0], later[0] * earlier[1] + later[1])


def on_device(
    resid,
    cotangent,
    routes,
    route_weight,
    w_gate,
    w_up,
    w_down,
    out_proj,
    gate_pre,
    log_decay,
    state_before,
    step_input,
):
    tok_rows, model_width = resid.shape
    top_count = routes.shape[1]
    groups = lax.axis_size("sp")
    capacity = 2 * tok_rows * top_count // groups
    flat_ids = routes.reshape(-1)
    onehot = (flat_ids[:, None] == jnp.arange(groups, dtype=jnp.int32)[None, :]).astype(jnp.int32)
    ranking = jnp.sum((jnp.cumsum(onehot, axis=0) - onehot) * onehot, axis=1)
    slot_ids = flat_ids * capacity + ranking
    member = slot_ids[None, :] == jnp.arange(groups * capacity, dtype=jnp.int32)[:, None]
    token_ids = jnp.arange(tok_rows * top_count, dtype=jnp.int32) // top_count
    filled = jnp.any(member, axis=1)
    slot_token = jnp.where(
        filled, jnp.sum(jnp.where(member, token_ids[None, :], 0), axis=1), tok_rows
    )
    slot_weight = jnp.sum(jnp.where(member, route_weight.reshape(-1)[None, :], 0.0), axis=1)
    col_width = model_width // lax.axis_size("tp")
    col_start = lax.axis_index("tp") * col_width
    cot_part = lax.dynamic_slice_in_dim(cotangent, col_start, col_width, 1)
    resid_part = lax.dynamic_slice_in_dim(resid, col_start, col_width, 1)
    send_rows, send_cot = gather_slots(
        resid_part, cot_part, slot_token, slot_weight, groups, capacity
    )
    got_rows, got_cot = (
        lax.all_to_all(send_rows, "sp", split_axis=0, concat_axis=0, tiled=True),
        lax.all_to_all(send_cot, "sp", split_axis=0, concat_axis=0, tiled=True),
    )
    full_rows, full_cot = (
        lax.all_gather(got_rows, "tp", axis=2, tiled=True),
        lax.all_gather(got_cot, "tp", axis=2, tiled=True),
    )
    grad_gate, grad_up, grad_down, partial_value = expert_work(
        full_rows.reshape(-1, model_width),
        full_cot.reshape(-1, model_width),
        w_gate[0],
        w_up[0],
        w_down[0],
    )
    summed = lax.psum_scatter(
        partial_value.reshape(groups, capacity, model_width).astype(jnp.bfloat16),
        "tp",
        scatter_dimension=2,
        tiled=True,
    )
    returned = lax.all_to_all(summed, "sp", split_axis=0, concat_axis=0, tiled=True)
    part_grad = combine_slots(returned, cot_part, slot_ids, tok_rows, top_count)
    resid_grad = lax.all_gather(part_grad, "tp", axis=1, tiled=True)
    decays = jnp.exp(log_decay)
    states = decays * state_before + step_input.astype(jnp.float32)
    gelu_val, gelu_back = jax.vjp(jax.nn.gelu, gate_pre.astype(jnp.float32))
    mixed = (gelu_val * states).astype(jnp.bfloat16)
    d_mixed = jnp.dot(resid_grad, out_proj, preferred_element_type=jnp.float32)
    grad_gate_pre = gelu_back(d_mixed * states)[0].astype(jnp.bfloat16)
    grad_proj = lax.psum_scatter(
        lax.dot_general(
            resid_grad, mixed, (((0,), (0,)), ((), ())), preferred_element_type=jnp.float32
        ).astype(jnp.bfloat16),
        "sp",
        scatter_dimension=0,
        tiled=True,
    ).astype(jnp.float32)
    direct = d_mixed * gelu_val
    channels = direct.shape[1]
    following = jnp.concatenate([decays[1:], jnp.ones((1, channels), jnp.float32)], axis=0)
    products, local_vals = lax.associative_scan(
        reverse_link, (jnp.flip(following, 0), jnp.flip(direct, 0)), axis=0
    )
    products = jnp.flip(products, 0)
    local_vals = jnp.flip(local_vals, 0)
    out_scale = decays[0] * products[0]
    out_shift = decays[0] * local_vals[0]
    identity = (jnp.ones((channels,), jnp.float32), jnp.zeros((channels,), jnp.float32))
    arriving = carried_in((out_scale, out_shift), "sp", compose, identity)
    grad_step_input = local_vals + products * arriving[1][None, :]
    grad_log_decay = grad_step_input * decays * state_before
    return (
        grad_gate,
        grad_up,
        grad_down,
        grad_proj,
        grad_gate_pre,
        grad_step_input,
        grad_log_decay,
    )


def solution(mesh):
    return jax.shard_map(
        on_device,
        mesh=mesh,
        in_specs=(
            P("sp", None),
            P("sp", None),
            P("sp", None),
            P("sp", None),
            P("sp", None, "tp"),
            P("sp", None, "tp"),
            P("sp", "tp", None),
            P(None, "tp"),
            P("sp", "tp"),
            P("sp", "tp"),
            P("sp", "tp"),
            P("sp", "tp"),
        ),
        out_specs=(
            P("sp", None, "tp"),
            P("sp", None, "tp"),
            P("sp", "tp", None),
            P("sp", "tp"),
            P("sp", "tp"),
            P("sp", "tp"),
            P("sp", "tp"),
        ),
        check_vma=False,
    )
```

profile of v0, /device:TPU:0, one launch (start us, length us, event | category | flops | bytes accessed | tf_op | source)
XLA Modules:
  0.0 636.2 jit_solution(3551452803279779135)
XLA Ops:
  14.0 5.4 gather_fusion
  19.4 44.4 %all_to_all.15 = bf16[8,192,512]{2,1,0:T(8,128)(2,1)} all-to-all(bf16[8,192,512]{2,1,0:T(8,128)(2,1)} %bitcast.63), channel_id=1, replica_groups=mesh['sp'=8,'tp'=4] {'sp'}, dimensions={0} | all-to-all | bytes 3145728 | tf_op jit(solution)/shard_map/all_to_all | solution.py:116
  64.9 5.4 gather_fusion.1
  73.2 40.2 %all_to_all.16 = bf16[8,192,512]{2,1,0:T(8,128)(2,1)} all-to-all(bf16[8,192,512]{2,1,0:T(8,128)(2,1)S(1)} %fusion.1), channel_id=1, replica_groups=mesh['sp'=8,'tp'=4] {'sp'}, dimensions={0} | all-to-all | bytes 3145728 | tf_op jit(solution)/shard_map/all_to_all | solution.py:117
  113.9 6.1 fusion.14
  123.0 35.9 %all-gather.8.cloned.1.call-done = bf16[8,192,2048]{2,1,0:T(8,128)(2,1)} async-done(((bf16[8,192,512]{2,1,0:T(8,128)(2,1)}), bf16[8,192,2048]{2,1,0:T(8,128)(2,1)}) %all-gather.8.cloned.1.call-update) | async-done | bytes 6291472 | tf_op jit(solution)/shard_map/all_gather | solution.py:121
  158.9 6.4 %multiply_convert_fusion.1 = (bf16[1536,256]{1,0:T(8,128)(2,1)S(1)}, bf16[1536,256]{1,0:T(8,128)(2,1)S(1)}) fusion(f32[1536,256]{1,0:T(8,128)} %fusion.14, f32[1536,256]{1,0:T(8,128)} %fusion.17, bf16[1536,2048]{1,0:T(8,128)(2,1)} %bitcast.72, bf16[1,256,2048]{2,1,0:T(8,128)(2,1)} %param.20), kind=kOutput, calls=%fused_computation.24 | convolution fusion | flops 1615724544 | bytes 12058624 | tf_op jit(solution)/shard_map/dot_general | solution.py:31
  171.7 58.0 %reduce-scatter.3.cloned.1.call-done = bf16[8,192,512]{2,1,0:T(8,128)(2,1)} async-done(((bf16[8,192,2048]{2,1,0:T(8,128)(2,1)}), bf16[8,192,512]{2,1,0:T(8,128)(2,1)}) %reduce-scatter.3.cloned.1.call-update) | async-done | bytes 1572880 | tf_op jit(solution)/shard_map/reduce_scatter | solution.py:130
  229.7 5.5 all-to-all-start.2
  235.2 12.0 %all-gather.10.cloned.1.call-start = ((), (), s32[]{:S(2)}) async-start(), calls=%async_computation.8 | async-start | bytes 1966080 | tf_op jit(solution)/shard_map/all_gather | solution.py:138
  247.6 24.6 %all-to-all-done.2 = bf16[8,192,512]{2,1,0:T(8,128)(2,1)} async-done(((bf16[8,192,512]{2,1,0:T(8,128)(2,1)}), bf16[8,192,512]{2,1,0:T(8,128)(2,1)}, u32[]{:S(2)}, u32[]{:S(2)}) %all-to-all-start.2) | async-done | bytes 1572896 | tf_op jit(solution)/shard_map/all_to_all | solution.py:136
  272.1 5.0 gather_fusion.2
  310.0 6.8 %slice.280 = f32[191,704]{1,0:T(8,128)} reverse(f32[191,704]{1,0:T(8,128)} %slice.279), dimensions={0} | reverse | bytes 1075712 | tf_op jit(solution)/shard_map/slice | solution.py:156
  316.8 6.7 %slice.289 = f32[192,704]{1,0:T(8,128)} reverse(f32[192,704]{1,0:T(8,128)} %slice.288), dimensions={0} | reverse | bytes 1081344 | tf_op jit(solution)/shard_map/slice | solution.py:156
  323.5 6.6 %slice.282 = f32[192,704]{1,0:T(8,128)} reverse(f32[192,704]{1,0:T(8,128)} %slice.281), dimensions={0} | reverse | bytes 1081344 | tf_op jit(solution)/shard_map/slice | solution.py:156
  330.1 6.3 convolution_bitcast_fusion.2
  336.4 6.2 convolution_bitcast_fusion.1
  356.9 6.6 %slice.286 = f32[192,704]{1,0:T(8,128)} reverse(f32[192,704]{1,0:T(8,128)} %slice.285), dimensions={0} | reverse | bytes 1081344 | tf_op jit(solution)/shard_map/slice | solution.py:156
  414.4 6.0 convolution_convert_fusion
  492.4 6.8 %slice.344 = f32[191,704]{1,0:T(8,128)} reverse(f32[191,704]{1,0:T(8,128)} %slice.343), dimensions={0} | reverse | bytes 1075712 | tf_op jit(solution)/shard_map/slice | solution.py:156
  521.9 9.9 %rev.9 = f32[384,704]{1,0:T(8,128)} reverse(f32[384,704]{1,0:T(8,128)} %add.308), dimensions={0} | reverse | bytes 2162688 | tf_op jit(solution)/shard_map/jit(_flip)/rev | solution.py:160
  543.0 9.8 %rev.10 = f32[384,704]{1,0:T(8,128)} reverse(f32[384,704]{1,0:T(8,128)} %add.316), dimensions={0} | reverse | bytes 2162688 | tf_op jit(solution)/shard_map/jit(_flip)/rev | solution.py:159
  553.7 30.5 %all-gather = f32[8,1,704]{2,1,0:T(1,128)S(1)} all-gather(f32[1,1,704]{2,1,0:T(1,128)S(1)} %get-tuple-element.121), channel_id=1, replica_groups=mesh['sp'=8,'tp'=4] {'sp'}, dimensions={0}, use_global_device_ids=true | all-gather | bytes 25344 | tf_op jit(solution)/shard_map/all_gather | solution.py:11
  584.2 30.5 %all-gather.1 = f32[8,1,704]{2,1,0:T(1,128)S(1)} all-gather(f32[1,1,704]{2,1,0:T(1,128)S(1)} %get-tuple-element.120), channel_id=1, replica_groups=mesh['sp'=8,'tp'=4] {'sp'}, dimensions={0}, use_global_device_ids=true | all-gather | bytes 25344 | tf_op jit(solution)/shard_map/all_gather | solution.py:11
  (294 shorter events, 240.0 us)
Async XLA Ops:
  7.2 338.7 %copy-start = (bf16[2048,704]{0,1:T(8,128)(2,1)S(1)}, bf16[2048,704]{0,1:T(8,128)(2,1)}, u32[]{:S(2)}) copy-start(bf16[2048,704]{0,1:T(8,128)(2,1)} %param.21) | copy-start | bytes 8650756
  7.2 106.7 %all-gather.6.cloned.1.call-start = ((), (), s32[]{:S(2)}) async-start(), calls=%async_computation.5 | async-start | bytes 7864320 | tf_op jit(solution)/shard_map/all_gather | solution.py:120
  63.8 95.1 %all-gather.8.cloned.1.call-start = ((), (), s32[]{:S(2)}) async-start(), calls=%async_computation.6 | async-start | bytes 7864320 | tf_op jit(solution)/shard_map/all_gather | solution.py:121
  113.4 116.3 %reduce-scatter.3.cloned.1.call-start = ((), (), s32[]{:S(2)}) async-start(), calls=%async_computation.7 | async-start | bytes 7864320 | tf_op jit(solution)/shard_map/reduce_scatter | solution.py:130
  158.9 6.4 %copy-start.16 = (bf16[1,2048,256]{2,1,0:T(8,128)(2,1)S(1)}, bf16[1,2048,256]{2,1,0:T(8,128)(2,1)}, u32[]{:S(2)}) copy-start(bf16[1,2048,256]{2,1,0:T(8,128)(2,1)} %param.18) | copy-start | bytes 3145732
  171.7 75.6 %copy-start.31 = (s32[384,2]{0,1:T(2,128)S(1)}, s32[384,2]{0,1:T(2,128)}, u32[]{:S(2)}) copy-start(s32[384,2]{0,1:T(2,128)} %param.16) | copy-start | bytes 9220
  229.7 42.5 %all-to-all-start.2 = ((bf16[8,192,512]{2,1,0:T(8,128)(2,1)}), bf16[8,192,512]{2,1,0:T(8,128)(2,1)}, u32[]{:S(2)}, u32[]{:S(2)}) async-start(bf16[8,192,512]{2,1,0:T(8,128)(2,1)} %reduce-scatter.3.cloned.1.call-done), calls=%async_computation.3 | async-start | bytes 3145728 | tf_op jit(solution)/shard_map/all_to_all | solution.py:136
  235.2 110.7 %all-gather.10.cloned.1.call-start = ((), (), s32[]{:S(2)}) async-start(), calls=%async_computation.8 | async-start | bytes 1966080 | tf_op jit(solution)/shard_map/all_gather | solution.py:138
  286.3 341.2 %reduce-scatter.5.cloned.1.call-start = ((), (), s32[]{:S(2)}) async-start(), calls=%async_computation.9 | async-start | bytes 3244032 | tf_op jit(solution)/shard_map/reduce_scatter | solution.py:145
  305.1 40.8 %copy-start.8 = (bf16[384,704]{1,0:T(8,128)(2,1)}, bf16[384,704]{1,0:T(8,128)(2,1)S(1)}, u32[]{:S(2)}) copy-start(bf16[384,704]{1,0:T(8,128)(2,1)S(1)} %copy.98) | copy-start | bytes 1622020
  330.1 6.3 copy-start.20
  330.1 12.5 %slice-start = ((s8[6291456]{0:T(1024)(128)(4,1)}), s8[4194304]{0:T(1024)(128)(4,1)S(1)}, s32[]{:S(2)}) async-start(s8[6291456]{0:T(1024)(128)(4,1)} %bitcast.73), calls=%async_computation.10 | async-start | bytes 8388608
  336.4 6.2 copy-start.36
  336.4 6.2 copy-start.37
  442.8 20.4 %copy-start.24 = (f32[5,704]{1,0:T(8,128)S(1)}, f32[5,704]{1,0:T(8,128)}, u32[]{:S(2)}) copy-start(f32[5,704]{1,0:T(8,128)} %slice.314) | copy-start | bytes 42244
  449.7 16.4 %copy-start.23 = (f32[11,704]{1,0:T(8,128)S(1)}, f32[11,704]{1,0:T(8,128)}, u32[]{:S(2)}) copy-start(f32[11,704]{1,0:T(8,128)} %slice.308) | copy-start | bytes 92932
  458.1 8.8 %copy-start.30 = (f32[1,704]{1,0:T(1,128)S(1)}, f32[1,704]{1,0:T(1,128)}, u32[]{:S(2)}) copy-start(f32[1,704]{1,0:T(1,128)} %slice.399) | copy-start | bytes 8452
  458.1 9.7 %copy-start.29 = (f32[1,704]{1,0:T(1,128)S(1)}, f32[1,704]{1,0:T(1,128)}, u32[]{:S(2)}) copy-start(f32[1,704]{1,0:T(1,128)} %slice.374) | copy-start | bytes 8452
  460.1 8.4 %copy-start.21 = (f32[23,704]{1,0:T(8,128)S(1)}, f32[23,704]{1,0:T(8,128)}, u32[]{:S(2)}) copy-start(f32[23,704]{1,0:T(8,128)} %slice.302) | copy-start | bytes 194308
  460.2 8.4 %copy-start.22 = (f32[23,704]{1,0:T(8,128)S(1)}, f32[23,704]{1,0:T(8,128)}, u32[]{:S(2)}) copy-start(f32[23,704]{1,0:T(8,128)} %slice.337) | copy-start | bytes 194308
  468.6 6.3 copy-start.28
  489.7 12.1 %copy-start.25 = (f32[1,704]{1,0:T(1,128)S(1)}, f32[1,704]{1,0:T(1,128)}, u32[]{:S(2)}) copy-start(f32[1,704]{1,0:T(1,128)} %slice.371) | copy-start | bytes 8452
  521.9 9.9 %copy-start.11 = (f32[191,704]{1,0:T(8,128)S(1)}, f32[191,704]{1,0:T(8,128)}, u32[]{:S(2)}) copy-start(f32[191,704]{1,0:T(8,128)} %get-tuple-element.122) | copy-start | bytes 1613572
  543.0 72.2 %copy-start.9 = (bf16[384,704]{1,0:T(8,128)(2,1)S(1)}, bf16[384,704]{1,0:T(8,128)(2,1)}, u32[]{:S(2)}) copy-start(bf16[384,704]{1,0:T(8,128)(2,1)} %copy-done.8) | copy-start | bytes 1622020
  (22 other events, 78.0 us)
Sparse Core Ops, SparseCore 0:
  63.9 45.3 all-gather.5
  113.5 45.3 all-gather.7
  171.8 57.8 reduce-scatter.2
  286.4 17.7 all-gather.9
  420.5 70.9 reduce-scatter.4
where the time goes:
time: 649 us; the launch traced here: 636 us
  local copies, waits for them, and re-layouts  227 us (35%)
  blocking collectives  146 us (22%)
  waiting for transfers between devices  119 us (18%)
  other arithmetic  63.8 us (10%)
  matrix products  47.8 us (7%)
  starting transfers between devices  18.1 us (3%)
  between operations  14.8 us (2%)
    slice x61, local copies, waits for them, and re-layouts, on_device(): lax.associative_scan(reverse_link, (jnp.flip(following, 0), jnp.flip(dire...  129 us
    all_gather x2, blocking collectives, carried_in(): gathered = jax.tree.map(lambda a: lax.all_gather(a, axis), part)  61 us
    reduce_scatter x1, waiting for transfers between devices, on_device(): lax.psum_scatter(partial_value.reshape(groups, capacity, model_width).ast...  58 us
    all_to_all x1, blocking collectives, on_device(): lax.all_to_all(send_rows, 'sp', split_axis=0, concat_axis=0, tiled=True)  44.4 us
    all_to_all x1, blocking collectives, on_device(): lax.all_to_all(send_cot, 'sp', split_axis=0, concat_axis=0, tiled=True)  40.2 us
    all_gather x1, waiting for transfers between devices, on_device(): lax.all_gather(got_cot, 'tp', axis=2, tiled=True)  35.9 us
    pad x30, local copies, waits for them, and re-layouts, on_device(): lax.associative_scan(reverse_link, (jnp.flip(following, 0), jnp.flip(dire...  33.1 us
    all_to_all x1, waiting for transfers between devices, on_device(): lax.all_to_all(summed, 'sp', split_axis=0, concat_axis=0, tiled=True)  24.6 us
  transfers between devices with their start and end apart: 6, of which 3 were waited for; matrix products, arithmetic and copies ran while one was open for 35% of the time, Pallas kernels for 0%

commit v1 on v0

--- a/solution.py
+++ b/solution.py
@@ -118,7 +118,7 @@
     )
     full_rows, full_cot = (
         lax.all_gather(got_rows, "tp", axis=2, tiled=True),
-        lax.all_gather(got_cot, "tp", axis=2, tiled=True),
+        jnp.concatenate(lax.all_gather(got_cot, "tp"), axis=2),
     )
     grad_gate, grad_up, grad_down, partial_value = expert_work(
         full_rows.reshape(-1, model_width),

time: 649 us -> 664 us (1.023)
  local copies, waits for them, and re-layouts: 227 us -> 244 us
  starting transfers between devices: 18.1 us -> 6.24 us
  waiting for transfers between devices: 119 us -> 130 us
    all_gather x1, starting transfers between devices: 12 us -> 0.04 us  [on_device(): resid_grad = lax.all_gather(part_grad, 'tp', axis=1, tiled=True)]
    all_to_all x1, waiting for transfers between devices: 24.6 us -> 36.5 us  [on_device(): lax.all_to_all(summed, 'sp', split_axis=0, concat_axis=0, tiled=True)]
    reshape x0 -> x1, local copies, waits for them, and re-layouts: none -> 10.3 us  [on_device(): jnp.concatenate(lax.all_gather(got_cot, 'tp'), axis=2)]
    unnamed x91 -> x96, local copies, waits for them, and re-layouts: 19.2 us -> 24.8 us
where the time goes in v1:
time: 664 us; the launch traced here: 652 us
  local copies, waits for them, and re-layouts  244 us (37%)
  blocking collectives  146 us (22%)
  waiting for transfers between devices  130 us (20%)
  other arithmetic  63.8 us (10%)
  matrix products  46.8 us (7%)
  between operations  14.8 us (2%)
    slice x61, local copies, waits for them, and re-layouts, on_device(): lax.associative_scan(reverse_link, (jnp.flip(following, 0), jnp.flip(dire...  129 us
    all_gather x2, blocking collectives, carried_in(): gathered = jax.tree.map(lambda a: lax.all_gather(a, axis), part)  61 us
    reduce_scatter x1, waiting for transfers between devices, on_device(): lax.psum_scatter(partial_value.reshape(groups, capacity, model_width).ast...  58 us
    all_to_all x1, blocking collectives, on_device(): lax.all_to_all(send_rows, 'sp', split_axis=0, concat_axis=0, tiled=True)  44.4 us
    all_to_all x1, blocking collectives, on_device(): lax.all_to_all(send_cot, 'sp', split_axis=0, concat_axis=0, tiled=True)  40.2 us
    all_to_all x1, waiting for transfers between devices, on_device(): lax.all_to_all(summed, 'sp', split_axis=0, concat_axis=0, tiled=True)  36.5 us
    all_gather x1, waiting for transfers between devices, on_device(): lax.all_gather(got_cot, 'tp')  35.7 us
    pad x30, local copies, waits for them, and re-layouts, on_device(): lax.associative_scan(reverse_link, (jnp.flip(following, 0), jnp.flip(dire...  33.1 us
  transfers between devices with their start and end apart: 6, of which 3 were waited for; matrix products, arithmetic and copies ran while one was open for 35% of the time, Pallas kernels for 0%

profile of v1, /device:TPU:0, one launch (start us, length us, event | category | flops | bytes accessed | tf_op | source)
XLA Modules:
  0.0 651.6 jit_solution(9764959079799711481)
XLA Ops:
  14.0 5.4 gather_fusion
  19.4 44.4 %all_to_all.15 = bf16[8,192,512]{2,1,0:T(8,128)(2,1)} all-to-all(bf16[8,192,512]{2,1,0:T(8,128)(2,1)} %bitcast.72), channel_id=1, replica_groups=mesh['sp'=8,'tp'=4] {'sp'}, dimensions={0} | all-to-all | bytes 3145728 | tf_op jit(solution)/shard_map/all_to_all | solution.py:116
  64.9 5.4 gather_fusion.1
  73.2 40.2 %all_to_all.16 = bf16[8,192,512]{2,1,0:T(8,128)(2,1)} all-to-all(bf16[8,192,512]{2,1,0:T(8,128)(2,1)S(1)} %fusion.1), channel_id=1, replica_groups=mesh['sp'=8,'tp'=4] {'sp'}, dimensions={0} | all-to-all | bytes 3145728 | tf_op jit(solution)/shard_map/all_to_all | solution.py:117
  114.0 6.1 fusion.14
  123.2 35.7 %all-gather.11.cloned.1.call-done = bf16[32,192,512]{2,1,0:T(8,128)(2,1)} async-done(((bf16[8,192,512]{2,1,0:T(8,128)(2,1)}), bf16[32,192,512]{2,1,0:T(8,128)(2,1)}) %all-gather.11.cloned.1.call-update) | async-done | bytes 6291472 | tf_op jit(solution)/shard_map/all_gather | solution.py:121
  158.9 10.3 %copy.106 = bf16[8,192,4,512]{3,2,1,0:T(4,128)(2,1)} copy(bf16[8,192,4,512]{3,1,0,2:T(8,128)(2,1)} %bitcast.70) | data formatting | bytes 12582912 | tf_op jit(solution)/shard_map/reshape | solution.py:121
  169.2 5.6 copy.121
  183.9 58.0 %reduce-scatter.3.cloned.1.call-done = bf16[8,192,512]{2,1,0:T(8,128)(2,1)} async-done(((bf16[8,192,2048]{2,1,0:T(8,128)(2,1)}), bf16[8,192,512]{2,1,0:T(8,128)(2,1)}) %reduce-scatter.3.cloned.1.call-update) | async-done | bytes 1572880 | tf_op jit(solution)/shard_map/reduce_scatter | solution.py:130
  241.9 5.5 all-to-all-start.2
  247.9 36.5 %all-to-all-done.2 = bf16[8,192,512]{2,1,0:T(8,128)(2,1)} async-done(((bf16[8,192,512]{2,1,0:T(8,128)(2,1)}), bf16[8,192,512]{2,1,0:T(8,128)(2,1)}, u32[]{:S(2)}, u32[]{:S(2)}) %all-to-all-start.2) | async-done | bytes 1572896 | tf_op jit(solution)/shard_map/all_to_all | solution.py:136
  322.5 6.8 %slice.280 = f32[191,704]{1,0:T(8,128)} reverse(f32[191,704]{1,0:T(8,128)} %slice.279), dimensions={0} | reverse | bytes 1075712 | tf_op jit(solution)/shard_map/slice | solution.py:156
  329.3 6.7 %slice.289 = f32[192,704]{1,0:T(8,128)} reverse(f32[192,704]{1,0:T(8,128)} %slice.288), dimensions={0} | reverse | bytes 1081344 | tf_op jit(solution)/shard_map/slice | solution.py:156
  335.9 6.6 %slice.282 = f32[192,704]{1,0:T(8,128)} reverse(f32[192,704]{1,0:T(8,128)} %slice.281), dimensions={0} | reverse | bytes 1081344 | tf_op jit(solution)/shard_map/slice | solution.py:156
  342.6 6.2 convolution_bitcast_fusion.2
  348.8 6.2 convolution_bitcast_fusion.1
  355.0 6.1 convolution_bitcast_fusion
  372.2 6.6 %slice.286 = f32[192,704]{1,0:T(8,128)} reverse(f32[192,704]{1,0:T(8,128)} %slice.285), dimensions={0} | reverse | bytes 1081344 | tf_op jit(solution)/shard_map/slice | solution.py:156
  429.7 6.0 convolution_convert_fusion
  507.8 6.8 %slice.344 = f32[191,704]{1,0:T(8,128)} reverse(f32[191,704]{1,0:T(8,128)} %slice.343), dimensions={0} | reverse | bytes 1075712 | tf_op jit(solution)/shard_map/slice | solution.py:156
  537.3 9.9 %rev.9 = f32[384,704]{1,0:T(8,128)} reverse(f32[384,704]{1,0:T(8,128)} %add.308), dimensions={0} | reverse | bytes 2162688 | tf_op jit(solution)/shard_map/jit(_flip)/rev | solution.py:160
  558.5 9.8 %rev.10 = f32[384,704]{1,0:T(8,128)} reverse(f32[384,704]{1,0:T(8,128)} %add.316), dimensions={0} | reverse | bytes 2162688 | tf_op jit(solution)/shard_map/jit(_flip)/rev | solution.py:159
  569.2 30.5 %all-gather.1 = f32[8,1,704]{2,1,0:T(1,128)S(1)} all-gather(f32[1,1,704]{2,1,0:T(1,128)S(1)} %get-tuple-element.121), channel_id=1, replica_groups=mesh['sp'=8,'tp'=4] {'sp'}, dimensions={0}, use_global_device_ids=true | all-gather | bytes 25344 | tf_op jit(solution)/shard_map/all_gather | solution.py:11
  599.7 30.5 %all-gather.2 = f32[8,1,704]{2,1,0:T(1,128)S(1)} all-gather(f32[1,1,704]{2,1,0:T(1,128)S(1)} %get-tuple-element.120), channel_id=1, replica_groups=mesh['sp'=8,'tp'=4] {'sp'}, dimensions={0}, use_global_device_ids=true | all-gather | bytes 25344 | tf_op jit(solution)/shard_map/all_gather | solution.py:11
  (299 shorter events, 245.1 us)
Async XLA Ops:
  7.2 353.9 %copy-start = (bf16[2048,704]{0,1:T(8,128)(2,1)S(1)}, bf16[2048,704]{0,1:T(8,128)(2,1)}, u32[]{:S(2)}) copy-start(bf16[2048,704]{0,1:T(8,128)(2,1)} %param.21) | copy-start | bytes 8650756
  7.2 106.8 %all-gather.7.cloned.1.call-start = ((), (), s32[]{:S(2)}) async-start(), calls=%async_computation.5 | async-start | bytes 7864320 | tf_op jit(solution)/shard_map/all_gather | solution.py:120
  63.8 95.1 %all-gather.11.cloned.1.call-start = ((), (), s32[]{:S(2)}) async-start(), calls=%async_computation.9 | async-start | bytes 7864320 | tf_op jit(solution)/shard_map/all_gather | solution.py:121
  113.4 128.6 %reduce-scatter.3.cloned.1.call-start = ((), (), s32[]{:S(2)}) async-start(), calls=%async_computation.6 | async-start | bytes 7864320 | tf_op jit(solution)/shard_map/reduce_scatter | solution.py:130
  114.0 6.2 copy-start.18
  114.0 6.2 copy-start.36
  183.9 63.6 %copy-start.32 = (s32[384,2]{0,1:T(2,128)S(1)}, s32[384,2]{0,1:T(2,128)}, u32[]{:S(2)}) copy-start(s32[384,2]{0,1:T(2,128)} %param.16) | copy-start | bytes 9220
  241.9 42.4 %all-to-all-start.2 = ((bf16[8,192,512]{2,1,0:T(8,128)(2,1)}), bf16[8,192,512]{2,1,0:T(8,128)(2,1)}, u32[]{:S(2)}, u32[]{:S(2)}) async-start(bf16[8,192,512]{2,1,0:T(8,128)(2,1)} %reduce-scatter.3.cloned.1.call-done), calls=%async_computation.3 | async-start | bytes 3145728 | tf_op jit(solution)/shard_map/all_to_all | solution.py:136
  247.5 113.6 %all-gather.9.cloned.1.call-start = ((), (), s32[]{:S(2)}) async-start(), calls=%async_computation.7 | async-start | bytes 1966080 | tf_op jit(solution)/shard_map/all_gather | solution.py:138
  298.5 344.4 %reduce-scatter.5.cloned.1.call-start = ((), (), s32[]{:S(2)}) async-start(), calls=%async_computation.8 | async-start | bytes 3244032 | tf_op jit(solution)/shard_map/reduce_scatter | solution.py:145
  317.5 43.6 %copy-start.9 = (bf16[384,704]{1,0:T(8,128)(2,1)}, bf16[384,704]{1,0:T(8,128)(2,1)S(1)}, u32[]{:S(2)}) copy-start(bf16[384,704]{1,0:T(8,128)(2,1)S(1)} %copy.108) | copy-start | bytes 1622020
  342.6 6.2 copy-start.21
  348.8 6.2 copy-start.39
  348.8 6.2 copy-start.41
  458.0 20.7 %copy-start.25 = (f32[5,704]{1,0:T(8,128)S(1)}, f32[5,704]{1,0:T(8,128)}, u32[]{:S(2)}) copy-start(f32[5,704]{1,0:T(8,128)} %slice.314) | copy-start | bytes 42244
  464.9 16.6 %copy-start.24 = (f32[11,704]{1,0:T(8,128)S(1)}, f32[11,704]{1,0:T(8,128)}, u32[]{:S(2)}) copy-start(f32[11,704]{1,0:T(8,128)} %slice.308) | copy-start | bytes 92932
  473.6 8.8 %copy-start.31 = (f32[1,704]{1,0:T(1,128)S(1)}, f32[1,704]{1,0:T(1,128)}, u32[]{:S(2)}) copy-start(f32[1,704]{1,0:T(1,128)} %slice.399) | copy-start | bytes 8452
  473.6 9.7 %copy-start.30 = (f32[1,704]{1,0:T(1,128)S(1)}, f32[1,704]{1,0:T(1,128)}, u32[]{:S(2)}) copy-start(f32[1,704]{1,0:T(1,128)} %slice.374) | copy-start | bytes 8452
  475.6 8.4 %copy-start.22 = (f32[23,704]{1,0:T(8,128)S(1)}, f32[23,704]{1,0:T(8,128)}, u32[]{:S(2)}) copy-start(f32[23,704]{1,0:T(8,128)} %slice.302) | copy-start | bytes 194308
  475.6 8.4 %copy-start.23 = (f32[23,704]{1,0:T(8,128)S(1)}, f32[23,704]{1,0:T(8,128)}, u32[]{:S(2)}) copy-start(f32[23,704]{1,0:T(8,128)} %slice.337) | copy-start | bytes 194308
  484.0 6.3 copy-start.29
  505.2 12.1 %copy-start.26 = (f32[1,704]{1,0:T(1,128)S(1)}, f32[1,704]{1,0:T(1,128)}, u32[]{:S(2)}) copy-start(f32[1,704]{1,0:T(1,128)} %slice.371) | copy-start | bytes 8452
  537.3 9.9 %copy-start.12 = (f32[191,704]{1,0:T(8,128)S(1)}, f32[191,704]{1,0:T(8,128)}, u32[]{:S(2)}) copy-start(f32[191,704]{1,0:T(8,128)} %get-tuple-element.122) | copy-start | bytes 1613572
  558.5 72.2 %copy-start.10 = (bf16[384,704]{1,0:T(8,128)(2,1)S(1)}, bf16[384,704]{1,0:T(8,128)(2,1)}, u32[]{:S(2)}) copy-start(bf16[384,704]{1,0:T(8,128)(2,1)} %copy-done.9) | copy-start | bytes 1622020
  (24 other events, 81.9 us)
Sparse Core Ops, SparseCore 0:
  63.9 45.3 all-gather.6
  113.5 45.3 all-gather.10
  184.0 57.8 reduce-scatter.2
  298.6 17.7 all-gather.8
  435.8 71.0 reduce-scatter.4
